TPU v7x, 32 devices: a whole 2x2x4 slice. The times are simulated.
32 devices in a mesh: grp: 2 (over y), fs: 4 (over z), tp: 4 (over x, core).
Axes of the slice: x: 2, y: 2, z: 4, core: 2. Of those that a mesh axis runs over, the one named last changes fastest.
Arguments:
- tokens: bfloat16 [8192, 2048], P(('grp', 'fs'), 'tp'), parts along dimension 0, may hold values from -50 to 50
- mix_gain: float32 [2048], replicated, may hold values from 0.1 to 1.9
- value_proj: bfloat16 [2048, 1024], P('fs', 'tp'), may hold values from -0.125 to 0.125
- gate_proj: bfloat16 [2048, 1024], P('fs', 'tp'), may hold values from -0.125 to 0.125
- conv_taps: float32 [31, 1024], P(None, 'tp'), may hold values from -1 to 1
- chan_gain: float32 [1024], replicated, may hold values from 0.1 to 1.9
- chan_shift: float32 [1024], replicated, may hold values from -3 to 3
- mix_out: bfloat16 [1024, 2048], P('fs', 'tp'), may hold values from -0.1875 to 0.1875
- mlp_gain: float32 [2048], replicated, may hold values from 0.1 to 1.9
- mlp_gate: bfloat16 [2048, 5632], P('fs', 'tp'), may hold values from -0.125 to 0.125
- mlp_up: bfloat16 [2048, 5632], P('fs', 'tp'), may hold values from -0.125 to 0.125
- gate_taps: float32 [3, 5632], P(None, 'tp'), may hold values from -3.5 to 3.5
- up_taps: float32 [3, 5632], P(None, 'tp'), may hold values from -3.5 to 3.5
- mlp_down: bfloat16 [5632, 2048], P('tp', 'fs'), may hold values from -0.078125 to 0.078125
- final_gain: float32 [2048], P('tp'), may hold values from 0.1 to 1.9
Outputs:
- layer_out: bfloat16 [8192, 2048], P(('grp', 'fs'), 'tp'), parts along dimension 0
There are 2 independent parts, one for each index of `grp`. A program takes and returns all parts, laid end to end along the dimension named above; an argument that names none is the same for every part. Nothing has to cross between parts.
All inputs are finite; a program needn't handle non-finite values.
Results may differ from a plain program's by a relative error of at most 0.0095.
Values may be sent and summed in bfloat16 or wider, within the bound.
A program may use at most 128 MiB of HBM per device.

v0:
```python
import jax
import jax.numpy as jnp
from jax import lax
from jax.sharding import PartitionSpec as P


def rms_scale(values, gain):
    return values * lax.rsqrt(jnp.mean(values * values, axis=-1, keepdims=True) + 1e-06) * gain


def along_sequence(values, taps):
    width = taps.shape[0]
    half = (width - 1) // 2
    length = values.shape[0]
    padded = jnp.pad(values, ((half, width - 1 - half), (0, 0)))
    total = jnp.zeros_like(values)
    for offset in range(width):
        total = total + taps[offset] * padded[offset : offset + length]
    return total


def local(
    tokens,
    mix_gain,
    value_proj,
    gate_proj,
    conv_taps,
    chan_gain,
    chan_shift,
    mix_out,
    mlp_gain,
    mlp_gate,
    mlp_up,
    gate_taps,
    up_taps,
    mlp_down,
    final_gain,
):
    width_tp = lax.axis_size("tp")
    whole = lax.all_gather(tokens, "tp", axis=1, tiled=True)
    normed = rms_scale(whole.astype(jnp.float32), mix_gain).astype(jnp.bfloat16)
    first = jnp.dot(
        normed,
        lax.all_gather(value_proj, "fs", axis=0, tiled=True),
        preferred_element_type=jnp.float32,
    )
    second = jnp.dot(
        normed,
        lax.all_gather(gate_proj, "fs", axis=0, tiled=True),
        preferred_element_type=jnp.float32,
    )
    glu = first * jax.nn.sigmoid(second)
    conv_out = along_sequence(glu, conv_taps).astype(jnp.bfloat16)
    own_channels = conv_out.shape[1]
    all_channels = own_channels * width_tp
    conv_wide = conv_out.astype(jnp.float32)
    totals = lax.psum(
        (
            jnp.sum(conv_wide, axis=-1, keepdims=True),
            jnp.sum(conv_wide * conv_wide, axis=-1, keepdims=True),
        ),
        "tp",
    )
    mean = totals[0] / all_channels
    var = totals[1] / all_channels - mean * mean
    offset_ch = lax.axis_index("tp") * own_channels
    gain_own = lax.dynamic_slice_in_dim(chan_gain, offset_ch, own_channels, 0)
    shift_own = lax.dynamic_slice_in_dim(chan_shift, offset_ch, own_channels, 0)
    chan_norm = (conv_wide - mean) * lax.rsqrt(var + 1e-05) * gain_own + shift_own
    hidden_own = jax.nn.silu(chan_norm).astype(jnp.bfloat16)
    hidden_mix = lax.all_gather(hidden_own, "tp", axis=1, tiled=True)
    mixer_result = jnp.dot(
        hidden_mix,
        lax.all_gather(mix_out, "fs", axis=0, tiled=True),
        preferred_element_type=jnp.float32,
    )
    mixed = (tokens.astype(jnp.float32) + mixer_result).astype(jnp.bfloat16)
    whole_two = lax.all_gather(mixed, "tp", axis=1, tiled=True)
    normed_two = rms_scale(whole_two.astype(jnp.float32), mlp_gain).astype(jnp.bfloat16)
    full_gate, full_up = (
        lax.all_gather(mlp_gate, "fs", axis=0, tiled=True),
        lax.all_gather(mlp_up, "fs", axis=0, tiled=True),
    )
    gate_pre = jnp.dot(normed_two, full_gate, preferred_element_type=jnp.float32)
    up_pre = jnp.dot(normed_two, full_up, preferred_element_type=jnp.float32)
    gate_conv = along_sequence(gate_pre, gate_taps)
    up_conv = along_sequence(up_pre, up_taps)
    hidden_mlp = (jax.nn.silu(gate_conv) * up_conv).astype(jnp.bfloat16)
    partial_terms = jnp.dot(
        hidden_mlp,
        lax.all_gather(mlp_down, "fs", axis=1, tiled=True),
        preferred_element_type=jnp.float32,
    )
    mlp_out = lax.psum_scatter(
        partial_terms.astype(jnp.bfloat16), "tp", scatter_dimension=1, tiled=True
    ).astype(jnp.float32)
    summed = mixed.astype(jnp.float32) + mlp_out
    squares = lax.psum(jnp.sum(summed * summed, axis=-1, keepdims=True), "tp")
    all_features = summed.shape[1] * width_tp
    layer_out = summed * lax.rsqrt(squares / all_features + 1e-06) * final_gain
    return layer_out.astype(jnp.bfloat16)


def solution(mesh):
    return jax.shard_map(
        local,
        mesh=mesh,
        in_specs=(
            P(("grp", "fs"), "tp"),
            P(),
            P("fs", "tp"),
            P("fs", "tp"),
            P(None, "tp"),
            P(),
            P(),
            P("fs", "tp"),
            P(),
            P("fs", "tp"),
            P("fs", "tp"),
            P(None, "tp"),
            P(None, "tp"),
            P("tp", "fs"),
            P("tp"),
        ),
        out_specs=P(("grp", "fs"), "tp"),
        check_vma=False,
    )
```

profile of v0, /device:TPU:0, one launch (start us, length us, event | category | flops | bytes accessed | tf_op | source)
XLA Modules:
  0.0 603.0 jit_solution(10716555549288945420)
XLA Ops:
  6.5 0.0 copy-start.5
  6.5 0.0 all-gather.10.cloned.1.call-start
  6.5 0.7 all-gather.10.cloned.1.call-update
  7.3 0.0 all-gather.14.cloned.1.call-start
  7.3 0.7 all-gather.14.cloned.1.call-update
  8.0 0.0 all-gather.12.cloned.1.call-start
  8.1 0.7 all-gather.12.cloned.1.call-update
  8.7 0.0 all-gather.18.cloned.1.call-start
  8.8 0.5 all-gather.18.cloned.1.call-update
  9.3 0.0 all-gather.16.cloned.1.call-start
  9.4 1.0 fusion.48
  10.4 1.1 fusion.49
  11.5 0.8 dynamic_slice.6
  12.2 0.8 dynamic_slice.7
  13.0 33.1 %all-gather.10.cloned.1.call-done = bf16[1024,2048]{1,0:T(8,128)(2,1)} async-done(((bf16[1024,512]{1,0:T(8,128)(2,1)}), bf16[1024,2048]{1,0:T(8,128)(2,1)}) %all-gather.10.cloned.1.call-update) | async-done | bytes 4194320 | tf_op jit(solution)/shard_map/all_gather | solution.py:40
  46.1 3.1 fusion
  49.2 26.5 %all-gather.14.cloned.1.call-done = bf16[2048,256]{1,0:T(8,128)(2,1)} async-done(((bf16[512,256]{1,0:T(8,128)(2,1)}), bf16[2048,256]{1,0:T(8,128)(2,1)}) %all-gather.14.cloned.1.call-update) | async-done | bytes 1048592 | tf_op jit(solution)/shard_map/all_gather | solution.py:49
  75.7 0.0 copy-done.5
  75.7 3.8 fusion.8
  79.5 0.0 copy-start.1
  79.5 25.1 %all-gather.12.cloned.1.call-done = bf16[2048,256]{1,0:T(8,128)(2,1)} async-done(((bf16[512,256]{1,0:T(8,128)(2,1)}), bf16[2048,256]{1,0:T(8,128)(2,1)}) %all-gather.12.cloned.1.call-update) | async-done | bytes 1048592 | tf_op jit(solution)/shard_map/all_gather | solution.py:44
  104.7 3.8 convolution_multiply_fusion
  108.5 4.6 convert_reduce_fusion
  113.1 6.6 %all-reduce.3 = (f32[1024,1]{0,1:T(1,128)S(1)}, f32[1024,1]{0,1:T(1,128)S(1)}) all-reduce(f32[1024,1]{0,1:T(1,128)S(1)} %bitcast.45, f32[1024,1]{0,1:T(1,128)S(1)} %bitcast.44), channel_id=1, replica_groups=mesh['grp'=2,'fs'=4,'tp'=4] {'tp'}, use_global_device_ids=true, to_apply=%region_4.5 | all-reduce | flops 2048 | bytes 16384 | tf_op jit(solution)/shard_map/psum | solution.py:57
  119.7 1.2 fusion.23
  121.0 0.0 all-gather.16.cloned.1.call-update
  121.0 0.0 all-gather.20.cloned.1.call-start
  121.0 0.0 copy-done.1
  121.0 0.5 copy.19
  121.6 0.0 copy-start.2
  121.6 0.0 copy-start.3
  121.6 11.9 %all-gather.18.cloned.1.call-done = bf16[1024,512]{1,0:T(8,128)(2,1)} async-done(((bf16[256,512]{1,0:T(8,128)(2,1)}), bf16[1024,512]{1,0:T(8,128)(2,1)}) %all-gather.18.cloned.1.call-update) | async-done | bytes 1048592 | tf_op jit(solution)/shard_map/all_gather | solution.py:74
  133.5 23.6 %all-gather.16.cloned.1.call-done = bf16[1024,1024]{1,0:T(8,128)(2,1)} async-done(((bf16[1024,256]{1,0:T(8,128)(2,1)}), bf16[1024,1024]{1,0:T(8,128)(2,1)}) %all-gather.16.cloned.1.call-update) | async-done | bytes 2097168 | tf_op jit(solution)/shard_map/all_gather | solution.py:71
  157.1 4.1 add_convert_fusion
  161.2 0.0 copy-start.6
  161.2 0.0 all-gather.20.cloned.1.call-update
  161.2 0.0 all-gather.22.cloned.1.call-start
  161.3 0.7 all-gather.22.cloned.1.call-update
  162.0 0.0 all-gather.24.cloned.1.call-start
  162.0 0.7 all-gather.24.cloned.1.call-update
  162.7 0.0 all-gather.26.cloned.1.call-start
  162.8 0.7 all-gather.26.cloned.1.call-update
  163.5 0.2 reduce-scatter.2.cloned.1.call-start
  163.7 0.0 copy-done.2
  163.7 0.0 copy-done.3
  163.7 0.1 slice_reduce_fusion.2
  163.8 32.0 %all-gather.20.cloned.1.call-done = bf16[1024,2048]{0,1:T(8,128)(2,1)} async-done(((bf16[1024,512]{0,1:T(8,128)(2,1)}), bf16[1024,2048]{0,1:T(8,128)(2,1)}) %all-gather.20.cloned.1.call-update) | async-done | bytes 4194320 | tf_op jit(solution)/shard_map/all_gather | solution.py:78
  195.9 3.1 fusion.3
  199.0 105.2 %all-gather.22.cloned.1.call-done = bf16[2048,1408]{1,0:T(8,128)(2,1)} async-done(((bf16[512,1408]{1,0:T(8,128)(2,1)}), bf16[2048,1408]{1,0:T(8,128)(2,1)}) %all-gather.22.cloned.1.call-update) | async-done | bytes 5767184 | tf_op jit(solution)/shard_map/all_gather | solution.py:81
  304.1 0.0 copy-done.6
  304.1 12.1 %fusion.11 = f32[1024,1408]{1,0:T(8,128)} fusion(bf16[2048,1408]{1,0:T(8,128)(2,1)} %all-gather.22.cloned.1.call-done, bf16[1024,2048]{0,1:T(8,128)(2,1)} %all-gather.20.cloned.1.call-done, f32[2048]{0:T(1024)S(1)} %copy-done.6, f32[1024]{0:T(1024)S(1)} %add_rsqrt_fusion.1), kind=kOutput, calls=%fused_computation.25 | convolution fusion | flops 5913968640 | bytes 15740928 | tf_op jit(solution)/shard_map/dot_general | solution.py:84
  316.2 94.4 %all-gather.24.cloned.1.call-done = bf16[2048,1408]{1,0:T(8,128)(2,1)} async-done(((bf16[512,1408]{1,0:T(8,128)(2,1)}), bf16[2048,1408]{1,0:T(8,128)(2,1)}) %all-gather.24.cloned.1.call-update) | async-done | bytes 5767184 | tf_op jit(solution)/shard_map/all_gather | solution.py:82
  410.7 12.0 %fusion.9 = f32[1024,1408]{1,0:T(8,128)} fusion(bf16[2048,1408]{1,0:T(8,128)(2,1)} %all-gather.24.cloned.1.call-done, bf16[1024,2048]{0,1:T(8,128)(2,1)} %all-gather.20.cloned.1.call-done, f32[2048]{0:T(1024)S(1)} %copy-done.6, f32[1024]{0:T(1024)S(1)} %add_rsqrt_fusion.1), kind=kOutput, calls=%fused_computation.24 | convolution fusion | flops 5913968640 | bytes 15740928 | tf_op jit(solution)/shard_map/dot_general | solution.py:85
  422.7 94.5 %all-gather.26.cloned.1.call-done = bf16[1408,2048]{1,0:T(8,128)(2,1)} async-done(((bf16[1408,512]{1,0:T(8,128)(2,1)}), bf16[1408,2048]{1,0:T(8,128)(2,1)}) %all-gather.26.cloned.1.call-update) | async-done | bytes 5767184 | tf_op jit(solution)/shard_map/all_gather | solution.py:91
  517.2 25.5 %convolution_convert_fusion = bf16[1024,2048]{0,1:T(8,128)(2,1)} fusion(bf16[1408,2048]{1,0:T(8,128)(2,1)} %all-gather.26.cloned.1.call-done, f32[1024,1408]{1,0:T(8,128)} %fusion.9, f32[1024,1408]{1,0:T(8,128)} %fusion.11, f32[1408]{0:T(1024)S(1)} %get-tuple-element.11, f32[1408]{0:T(1024)S(1)} %get-tuple-element.12, f32[1408]{0:T(1024)S(1)} %get-tuple-element.10, ...), kind=kOutput, calls=%fused_computation.11 | convolution fusion | flops 5930745856 | bytes 21529600 | tf_op jit(solution)/shard_map/dot_general | solution.py:89
  542.8 0.0 copy-start.4
  542.8 0.0 reduce-scatter.2.cloned.1.call-update
  542.8 43.0 %reduce-scatter.2.cloned.1.call-done = bf16[1024,512]{0,1:T(8,128)(2,1)} async-done(((bf16[1024,2048]{0,1:T(8,128)(2,1)}), bf16[1024,512]{0,1:T(8,128)(2,1)}) %reduce-scatter.2.cloned.1.call-update) | async-done | bytes 1048592 | tf_op jit(solution)/shard_map/reduce_scatter | solution.py:94
  585.8 0.0 copy-done
  585.8 1.6 multiply_reduce_fusion
  587.4 5.8 psum.23
  593.2 0.0 copy-done.4
  593.2 1.6 multiply_convert_fusion.2
  594.8 1.3 copy.21
  (5 shorter events, 0.1 us)
Async XLA Ops:
  6.5 69.2 %copy-start.5 = (f32[2048]{0:T(1024)S(1)}, f32[2048]{0:T(1024)}, u32[]{:S(2)}) copy-start(f32[2048]{0:T(1024)} %param.16) | copy-start | bytes 24580
  6.5 39.6 %all-gather.10.cloned.1.call-start = ((), (), s32[]{:S(2)}) async-start(), calls=%async_computation.1 | async-start | bytes 5242880 | tf_op jit(solution)/shard_map/all_gather | solution.py:40
  7.3 68.4 %all-gather.14.cloned.1.call-start = ((), (), s32[]{:S(2)}) async-start(), calls=%async_computation.3 | async-start | bytes 1310720 | tf_op jit(solution)/shard_map/all_gather | solution.py:49
  8.0 96.7 %all-gather.12.cloned.1.call-start = ((), (), s32[]{:S(2)}) async-start(), calls=%async_computation.2 | async-start | bytes 1310720 | tf_op jit(solution)/shard_map/all_gather | solution.py:44
  8.7 124.7 %all-gather.18.cloned.1.call-start = ((), (), s32[]{:S(2)}) async-start(), calls=%async_computation.5 | async-start | bytes 1310720 | tf_op jit(solution)/shard_map/all_gather | solution.py:74
  9.3 147.8 %all-gather.16.cloned.1.call-start = ((), (), s32[]{:S(2)}) async-start(), calls=%async_computation.4 | async-start | bytes 2621440 | tf_op jit(solution)/shard_map/all_gather | solution.py:71
  79.5 41.5 %copy-start.1 = (bf16[1024,512]{1,0:T(8,128)(2,1)S(1)}, bf16[1024,512]{1,0:T(8,128)(2,1)}, u32[]{:S(2)}) copy-start(bf16[1024,512]{1,0:T(8,128)(2,1)} %param.15) | copy-start | bytes 3145732
  121.0 74.9 %all-gather.20.cloned.1.call-start = ((), (), s32[]{:S(2)}) async-start(), calls=%async_computation.6 | async-start | bytes 5242880 | tf_op jit(solution)/shard_map/all_gather | solution.py:78
  121.6 42.1 %copy-start.2 = (f32[3,1408]{1,0:T(4,128)S(1)}, f32[3,1408]{1,0:T(4,128)}, u32[]{:S(2)}) copy-start(f32[3,1408]{1,0:T(4,128)} %param.27) | copy-start | bytes 50692
  121.6 42.1 %copy-start.3 = (f32[3,1408]{1,0:T(4,128)S(1)}, f32[3,1408]{1,0:T(4,128)}, u32[]{:S(2)}) copy-start(f32[3,1408]{1,0:T(4,128)} %param.26) | copy-start | bytes 50692
  161.2 142.9 %copy-start.6 = (f32[2048]{0:T(1024)S(1)}, f32[2048]{0:T(1024)}, u32[]{:S(2)}) copy-start(f32[2048]{0:T(1024)} %param.23) | copy-start | bytes 24580
  161.2 142.9 %all-gather.22.cloned.1.call-start = ((), (), s32[]{:S(2)}) async-start(), calls=%async_computation.7 | async-start | bytes 7208960 | tf_op jit(solution)/shard_map/all_gather | solution.py:81
  162.0 248.7 %all-gather.24.cloned.1.call-start = ((), (), s32[]{:S(2)}) async-start(), calls=%async_computation.8 | async-start | bytes 7208960 | tf_op jit(solution)/shard_map/all_gather | solution.py:82
  162.7 354.5 %all-gather.26.cloned.1.call-start = ((), (), s32[]{:S(2)}) async-start(), calls=%async_computation.9 | async-start | bytes 7208960 | tf_op jit(solution)/shard_map/all_gather | solution.py:91
  163.5 422.3 %reduce-scatter.2.cloned.1.call-start = ((), (), s32[]{:S(2)}) async-start(), calls=%async_computation.10 | async-start | bytes 5242880 | tf_op jit(solution)/shard_map/reduce_scatter | solution.py:94
  517.2 68.6 %copy-start = (bf16[1024,512]{0,1:T(8,128)(2,1)S(1)}, bf16[1024,512]{0,1:T(8,128)(2,1)}, u32[]{:S(2)}) copy-start(bf16[1024,512]{0,1:T(8,128)(2,1)} %add_convert_fusion) | copy-start | bytes 3145732
  542.8 50.4 %copy-start.4 = (f32[512]{0:T(512)S(1)}, f32[512]{0:T(512)}, u32[]{:S(2)}) copy-start(f32[512]{0:T(512)} %param.29) | copy-start | bytes 6148
Sparse Core Ops, SparseCore 0:
  8.9 37.1 all-gather.9
  47.7 27.9 all-gather.13
  77.3 27.3 all-gather.11
  106.1 27.3 all-gather.17
  134.9 22.1 all-gather.15
  161.4 34.4 all-gather.19
  197.4 106.6 all-gather.21
  305.7 104.9 all-gather.23
  412.3 104.9 all-gather.25
  542.9 42.8 reduce-scatter.1
where the time goes:
time: 603 us
  waiting for transfers between devices  494 us (82%)
  matrix products  61.4 us (10%)
  other arithmetic  15.3 us (3%)
  between operations  13.7 us (2%)
  blocking collectives  12.4 us (2%)
    all_gather x1, waiting for transfers between devices, local(): lax.all_gather(mlp_gate, 'fs', axis=0, tiled=True)  105 us
    all_gather x1, waiting for transfers between devices, local(): lax.all_gather(mlp_down, 'fs', axis=1, tiled=True)  94.5 us
    all_gather x1, waiting for transfers between devices, local(): lax.all_gather(mlp_up, 'fs', axis=0, tiled=True)  94.4 us
    reduce_scatter x1, waiting for transfers between devices, local(): lax.psum_scatter(partial_terms.astype(jnp.bfloat16), 'tp', scatter_dimens...  43 us
    all_gather x1, waiting for transfers between devices, local(): whole = lax.all_gather(tokens, 'tp', axis=1, tiled=True)  33.1 us
    all_gather x1, waiting for transfers between devices, local(): whole_two = lax.all_gather(mixed, 'tp', axis=1, tiled=True)  32 us
    all_gather x1, waiting for transfers between devices, local(): lax.all_gather(gate_proj, 'fs', axis=0, tiled=True)  26.5 us
    dot_general x1, matrix products, local(): jnp.dot(hidden_mlp, lax.all_gather(mlp_down, 'fs', axis=1, tiled=True), p...  25.5 us
  transfers between devices with their start and end apart: 10, of which 10 were waited for; matrix products, arithmetic and copies ran while one was open for 8% of the time, Pallas kernels for 0%

commit v1 on v0

v1 whole, which is shorter than its diff:
```python
import jax
import jax.numpy as jnp
from jax import lax
from jax.sharding import PartitionSpec as P


DOWN_PIECES = 2
SUM_CHUNKS = 2


def along_sequence(values, taps):
    width = taps.shape[0]
    half = (width - 1) // 2
    length = values.shape[0]
    padded = jnp.pad(values, ((half, width - 1 - half), (0, 0)))
    total = jnp.zeros_like(values)
    for offset in range(width):
        total = total + taps[offset] * padded[offset : offset + length]
    return total


def put(whole, piece, index):
    return lax.dynamic_update_slice_in_dim(whole, piece[None], index, 0)


def take(parts, index, axis=0):
    return lax.dynamic_index_in_dim(parts, index, axis, keepdims=False)


def shifted(value, axis, shift):
    size = lax.axis_size(axis)
    return lax.ppermute(value, axis, [(i, (i + shift) % size) for i in range(size)])


def swapped(value, mask):
    size = lax.axis_size("tp")
    return lax.ppermute(value, "tp", [(i, i ^ mask) for i in range(size)])


def masks_of_size(size):
    assert size & (size - 1) == 0
    return [1 << bit for bit in range(size.bit_length() - 1)]


def masks_of(axis):
    return masks_of_size(lax.axis_size(axis))


def gathered_features(own):
    me = lax.axis_index("tp")
    whole = put(jnp.zeros((lax.axis_size("tp"),) + own.shape, own.dtype), own, me)
    held = [(0, own)]
    for mask in reversed(masks_of("tp")):
        for code, block in held[:]:
            held.append((code ^ mask, swapped(block, mask)))
    for code, block in held[1:]:
        whole = put(whole, block, me ^ code)
    return whole


def scattered_sum(blocks, first, count):
    me = lax.axis_index("tp")
    k, columns = blocks.shape[1], blocks.shape[3]

    def block(index):
        piece = lax.dynamic_slice(blocks, (index, 0, first, 0), (1, k, count, columns))
        return piece.reshape(k * count, columns)

    keep, send = None, None
    for mask in masks_of("tp"):
        bit = (me // mask) % 2
        if keep is None:
            half = range(blocks.shape[0] // 2)
            send = [block(2 * i + 1 - bit) for i in half]
            keep = [block(2 * i + bit) for i in half]
        else:
            pairs = list(zip(sums[0::2], sums[1::2]))
            send = [jnp.where(bit == 1, low, high).astype(jnp.bfloat16) for low, high in pairs]
            keep = [jnp.where(bit == 1, high, low) for low, high in pairs]
        sums = [
            own.astype(jnp.float32) + swapped(other, mask).astype(jnp.float32)
            for own, other in zip(keep, send)
        ]
    return sums[0].reshape(k, count, columns)


def parts_of(shard, pieces=1):
    count = lax.axis_size("grp") * pieces
    return shard.reshape(count, shard.shape[0] // count, shard.shape[1])


def shards_by_arrival(shard, pieces=1):
    groups = lax.axis_size("grp")
    group = lax.axis_index("grp")
    parts = parts_of(shard, pieces)
    arrived = [None]
    moving = [take(parts, group * pieces + i) for i in range(pieces)]
    for _ in range(1, lax.axis_size("fs")):
        got = []
        for i in range(pieces):
            moving[i] = shifted(moving[i], "fs", 1)
            got.append((group * pieces + i, moving[i]))
            for jump in range(1, groups):
                other = shifted(moving[i], "grp", jump)
                got.append(((group - jump) % groups * pieces + i, other))
        arrived.append(got)
    return arrived


def gathered_rows(shard):
    size = lax.axis_size("fs")
    groups = lax.axis_size("grp")
    me = lax.axis_index("fs")
    parts = parts_of(shard)
    whole = jnp.zeros((size * groups,) + parts.shape[1:], shard.dtype)
    whole = lax.dynamic_update_slice_in_dim(whole, parts, me * groups, 0)
    for step, got in enumerate(shards_by_arrival(shard)):
        for part, piece in got or ():
            whole = put(whole, piece, (me - step) % size * groups + part)
    return whole.reshape(size * shard.shape[0], shard.shape[1])


def over_blocks(blocks, weight):
    weight = weight.reshape(blocks.shape[0], blocks.shape[2], weight.shape[1])
    return jnp.einsum("btk,bkn->tn", blocks, weight, preferred_element_type=jnp.float32)


def normed_blocks(blocks, gain):
    values = blocks.astype(jnp.float32)
    mean = jnp.mean(values * values, axis=(0, 2), keepdims=True)
    gain = gain.reshape(blocks.shape[0], 1, blocks.shape[2])
    return (values * lax.rsqrt(mean + 1e-06) * gain).astype(jnp.bfloat16)


def local(
    tokens,
    mix_gain,
    value_proj,
    gate_proj,
    conv_taps,
    chan_gain,
    chan_shift,
    mix_out,
    mlp_gain,
    mlp_gate,
    mlp_up,
    gate_taps,
    up_taps,
    mlp_down,
    final_gain,
):
    width_tp = lax.axis_size("tp")
    size_fs = lax.axis_size("fs")
    me_fs = lax.axis_index("fs")
    rows = tokens.shape[0]
    whole = gathered_features(tokens)
    full_in = gathered_rows(jnp.concatenate([value_proj, gate_proj], axis=1))
    full_mix = gathered_rows(mix_out)
    full_gate = gathered_rows(mlp_gate)
    full_up = gathered_rows(mlp_up)
    down_shards = shards_by_arrival(mlp_down, DOWN_PIECES)
    both = over_blocks(normed_blocks(whole, mix_gain), full_in)
    own_channels = value_proj.shape[1]
    glu = both[:, :own_channels] * jax.nn.sigmoid(both[:, own_channels:])
    conv_out = along_sequence(glu, conv_taps).astype(jnp.bfloat16)
    all_channels = own_channels * width_tp
    conv_wide = conv_out.astype(jnp.float32)
    totals = lax.psum(
        (
            jnp.sum(conv_wide, axis=-1, keepdims=True),
            jnp.sum(conv_wide * conv_wide, axis=-1, keepdims=True),
        ),
        "tp",
    )
    mean = totals[0] / all_channels
    var = totals[1] / all_channels - mean * mean
    offset_ch = lax.axis_index("tp") * own_channels
    gain_own = lax.dynamic_slice_in_dim(chan_gain, offset_ch, own_channels, 0)
    shift_own = lax.dynamic_slice_in_dim(chan_shift, offset_ch, own_channels, 0)
    chan_norm = (conv_wide - mean) * lax.rsqrt(var + 1e-05) * gain_own + shift_own
    hidden_own = jax.nn.silu(chan_norm).astype(jnp.bfloat16)
    hidden_mix = gathered_features(hidden_own)
    mixer_result = over_blocks(hidden_mix, full_mix)
    mixed = (tokens.astype(jnp.float32) + mixer_result).astype(jnp.bfloat16)
    normed_two = normed_blocks(gathered_features(mixed), mlp_gain)
    gate_conv = along_sequence(over_blocks(normed_two, full_gate), gate_taps)
    up_conv = along_sequence(over_blocks(normed_two, full_up), up_taps)
    hidden_mlp = (jax.nn.silu(gate_conv) * up_conv).astype(jnp.bfloat16)
    hidden_mlp = lax.optimization_barrier(hidden_mlp)
    partial_terms = jnp.zeros((size_fs, rows, mlp_down.shape[1]), jnp.bfloat16)
    for step, got in enumerate(down_shards):
        weight = mlp_down
        if got:
            weight = jnp.zeros(parts_of(mlp_down, DOWN_PIECES).shape, mlp_down.dtype)
            for part, piece in got:
                weight = put(weight, piece, part)
            weight = weight.reshape(mlp_down.shape)
        columns = jnp.dot(hidden_mlp, weight, preferred_element_type=jnp.float32)
        partial_terms = put(partial_terms, columns.astype(jnp.bfloat16), (me_fs - step) % size_fs)
    per_owner = size_fs // width_tp
    assert per_owner * width_tp == size_fs
    partial_terms = partial_terms.reshape(width_tp, per_owner, rows, mlp_down.shape[1])
    chunk = rows // SUM_CHUNKS
    sums = [
        scattered_sum(partial_terms, i * chunk, chunk) for i in range(SUM_CHUNKS)
    ]
    mlp_out = jnp.moveaxis(jnp.concatenate(sums, axis=1), 0, 1).reshape(mixed.shape)
    summed = mixed.astype(jnp.float32) + mlp_out
    squares = lax.psum(jnp.sum(summed * summed, axis=-1, keepdims=True), "tp")
    all_features = summed.shape[1] * width_tp
    layer_out = summed * lax.rsqrt(squares / all_features + 1e-06) * final_gain
    return layer_out.astype(jnp.bfloat16)


def solution(mesh):
    return jax.shard_map(
        local,
        mesh=mesh,
        in_specs=(
            P(("grp", "fs"), "tp"),
            P(),
            P("fs", "tp"),
            P("fs", "tp"),
            P(None, "tp"),
            P(),
            P(),
            P("fs", "tp"),
            P(),
            P("fs", "tp"),
            P("fs", "tp"),
            P(None, "tp"),
            P(None, "tp"),
            P("tp", "fs"),
            P("tp"),
        ),
        out_specs=P(("grp", "fs"), "tp"),
        check_vma=False,
    )
```

time: 603 us -> 402 us (0.67); the launches traced: 603 us -> 395 us
  waiting for transfers between devices: 494 us -> 191 us
  local copies, waits for them, and re-layouts: 5.61 us -> 84.3 us
  starting transfers between devices: 0.53 us -> 37.9 us
  matrix products: 61.4 us -> 38.1 us
  other arithmetic: 15.3 us -> 29.8 us
  between operations: 13.7 us -> 1.42 us
    all_gather x9 -> x0, waiting for transfers between devices: 446 us -> none  [the longest x1 105 us: local(): lax.all_gather(mlp_gate, 'fs', axis=0, tiled=True)]
    ppermute x0 -> x51, waiting for transfers between devices: none -> 191 us  [the longest x36 154 us: shifted(): lax.ppermute(value, axis, [(i, (i + shift) % size) for i in range(size)])]
    reduce_scatter x1 -> x0, waiting for transfers between devices: 43 us -> none  [local(): lax.psum_scatter(partial_terms.astype(jnp.bfloat16), 'tp', scatter_dimens...]
    dynamic_update_slice x0 -> x50, local copies, waits for them, and re-layouts: none -> 40.7 us  [the longest x46 37.4 us: put(): return lax.dynamic_update_slice_in_dim(whole, piece[None], index, 0)]
    ppermute x0 -> x51, starting transfers between devices: none -> 37.9 us  [the longest x36 30.5 us: shifted(): lax.ppermute(value, axis, [(i, (i + shift) % size) for i in range(size)])]
    dot_general x6 -> x8, matrix products: 61.4 us -> 38.1 us  [the longest x4 29.4 us: over_blocks(): jnp.einsum('btk,bkn->tn', blocks, weight, preferred_element_type=jnp.floa...]
    convert_element_type x1 -> x2, other arithmetic: 1.24 us -> 13.3 us  [the longest x1 11.1 us: local(): hidden_mlp = (jax.nn.silu(gate_conv) * up_conv).astype(jnp.bfloat16)]
    another operation x0 -> x7, local copies, waits for them, and re-layouts: none -> 11.9 us
  transfers between devices with their start and end apart: 10 -> 51, of which waited for: 10 -> 27; matrix products, arithmetic and copies ran while one was open for 8% -> 23% of each run, Pallas kernels for 0% -> 0%
where the time goes in v1:
time: 402 us; the launch traced here: 395 us
  waiting for transfers between devices  191 us (48%)
  local copies, waits for them, and re-layouts  84.3 us (21%)
  matrix products  38.1 us (9%)
  starting transfers between devices  37.9 us (9%)
  other arithmetic  29.8 us (7%)
  blocking collectives  12.3 us (3%)
    ppermute x36, waiting for transfers between devices, shifted(): lax.ppermute(value, axis, [(i, (i + shift) % size) for i in range(size)])  154 us
    dynamic_update_slice x46, local copies, waits for them, and re-layouts, put(): return lax.dynamic_update_slice_in_dim(whole, piece[None], index, 0)  37.4 us
    ppermute x15, waiting for transfers between devices, swapped(): return lax.ppermute(value, 'tp', [(i, i ^ mask) for i in range(size)])  36.6 us
    ppermute x36, starting transfers between devices, shifted(): lax.ppermute(value, axis, [(i, (i + shift) % size) for i in range(size)])  30.5 us
    dot_general x4, matrix products, over_blocks(): jnp.einsum('btk,bkn->tn', blocks, weight, preferred_element_type=jnp.floa...  29.4 us
    another operation x7, local copies, waits for them, and re-layouts  11.9 us
    convert_element_type x1, other arithmetic, local(): hidden_mlp = (jax.nn.silu(gate_conv) * up_conv).astype(jnp.bfloat16)  11.1 us
    dot_general x4, matrix products, local(): columns = jnp.dot(hidden_mlp, weight, preferred_element_type=jnp.float32)  8.69 us
  transfers between devices with their start and end apart: 51, of which 27 were waited for; matrix products, arithmetic and copies ran while one was open for 23% of the time, Pallas kernels for 0%

profile of v1, /device:TPU:0, one launch (start us, length us, event | category | flops | bytes accessed | tf_op | source)
XLA Modules:
  0.0 394.7 jit_solution(13247283256226744926)
XLA Ops:
  0.0 3.0 collective-permute-start
  4.8 1.6 collective-permute-start.3
  7.9 1.6 collective-permute-start.12
  9.5 2.0 dynamic-slice_bitcast_fusion.1
  13.1 1.7 fusion.61
  14.8 1.6 fusion.62
  23.6 2.9 broadcast.75.clone.1
  28.7 2.9 broadcast.75.clone
  33.4 2.3 broadcast.70.clone
  36.8 1.6 slice_reduce_fusion.2
  39.6 1.6 collective-permute-start.13
  41.8 2.9 collective-permute-done.13
  47.1 5.7 %collective-permute-done.14 = bf16[128,512]{1,0:T(8,128)(2,1)S(1)} collective-permute-done((bf16[128,512]{1,0:T(8,128)(2,1)S(1)}, bf16[128,512]{1,0:T(8,128)(2,1)S(1)}, u32[]{:S(2)}, u32[]{:S(2)}) %collective-permute-start.14) | collective-permute-done | bytes 131104 | tf_op jit(solution)/shard_map/ppermute | solution.py:32
  55.0 3.3 collective-permute-done.33
  60.0 3.3 collective-permute-done.15
  64.0 6.1 %collective-permute-done.16 = bf16[128,512]{1,0:T(8,128)(2,1)S(1)} collective-permute-done((bf16[128,512]{1,0:T(8,128)(2,1)S(1)}, bf16[128,512]{1,0:T(8,128)(2,1)S(1)}, u32[]{:S(2)}, u32[]{:S(2)}) %collective-permute-start.16) | collective-permute-done | bytes 131104 | tf_op jit(solution)/shard_map/ppermute | solution.py:32
  70.8 10.3 %collective-permute-done.5 = bf16[256,512]{1,0:T(8,128)(2,1)S(1)} collective-permute-done((bf16[256,512]{1,0:T(8,128)(2,1)S(1)}, bf16[256,512]{1,0:T(8,128)(2,1)S(1)}, u32[]{:S(2)}, u32[]{:S(2)}) %collective-permute-start.5) | collective-permute-done | bytes 262176 | tf_op jit(solution)/shard_map/ppermute | solution.py:32
  82.6 3.4 collective-permute-done.17
  88.2 2.0 bitcast_dynamic-update-slice_fusion.15
  90.2 9.5 %collective-permute-done.35 = bf16[352,512]{1,0:T(8,128)(2,1)S(1)} collective-permute-done((bf16[352,512]{1,0:T(8,128)(2,1)S(1)}, bf16[352,512]{1,0:T(8,128)(2,1)S(1)}, u32[]{:S(2)}, u32[]{:S(2)}) %collective-permute-start.35) | collective-permute-done | bytes 360480 | tf_op jit(solution)/shard_map/ppermute | solution.py:32
  102.2 10.6 %collective-permute-done.37 = bf16[352,512]{1,0:T(8,128)(2,1)S(1)} collective-permute-done((bf16[352,512]{1,0:T(8,128)(2,1)S(1)}, bf16[352,512]{1,0:T(8,128)(2,1)S(1)}, u32[]{:S(2)}, u32[]{:S(2)}) %collective-permute-start.37) | collective-permute-done | bytes 360480 | tf_op jit(solution)/shard_map/ppermute | solution.py:32
  114.6 7.4 %collective-permute-done.6 = bf16[256,512]{1,0:T(8,128)(2,1)S(1)} collective-permute-done((bf16[256,512]{1,0:T(8,128)(2,1)S(1)}, bf16[256,512]{1,0:T(8,128)(2,1)S(1)}, u32[]{:S(2)}, u32[]{:S(2)}) %collective-permute-start.6) | collective-permute-done | bytes 262176 | tf_op jit(solution)/shard_map/ppermute | solution.py:32
  123.5 2.0 collective-permute-done.7
  125.9 2.3 bitcast_dynamic-update-slice_fusion.2
  128.2 16.0 %collective-permute-done.8 = bf16[256,512]{1,0:T(8,128)(2,1)S(1)} collective-permute-done((bf16[256,512]{1,0:T(8,128)(2,1)S(1)}, bf16[256,512]{1,0:T(8,128)(2,1)S(1)}, u32[]{:S(2)}, u32[]{:S(2)}) %collective-permute-start.8) | collective-permute-done | bytes 262176 | tf_op jit(solution)/shard_map/ppermute | solution.py:32
  146.2 2.3 bitcast_dynamic-update-slice_fusion.1
  148.5 6.9 %collective-permute-done.38 = bf16[352,512]{1,0:T(8,128)(2,1)S(1)} collective-permute-done((bf16[352,512]{1,0:T(8,128)(2,1)S(1)}, bf16[352,512]{1,0:T(8,128)(2,1)S(1)}, u32[]{:S(2)}, u32[]{:S(2)}) %collective-permute-start.38) | collective-permute-done | bytes 360480 | tf_op jit(solution)/shard_map/ppermute | solution.py:32
  157.0 10.7 %collective-permute-done.40 = bf16[352,512]{1,0:T(8,128)(2,1)S(1)} collective-permute-done((bf16[352,512]{1,0:T(8,128)(2,1)S(1)}, bf16[352,512]{1,0:T(8,128)(2,1)S(1)}, u32[]{:S(2)}, u32[]{:S(2)}) %collective-permute-start.40) | collective-permute-done | bytes 360480 | tf_op jit(solution)/shard_map/ppermute | solution.py:32
  170.8 17.6 %collective-permute-done.43 = bf16[352,512]{1,0:T(8,128)(2,1)} collective-permute-done((bf16[352,512]{1,0:T(8,128)(2,1)S(1)}, bf16[352,512]{1,0:T(8,128)(2,1)}, u32[]{:S(2)}, u32[]{:S(2)}) %collective-permute-start.43) | collective-permute-done | bytes 360480 | tf_op jit(solution)/shard_map/ppermute | solution.py:32
  190.5 2.0 bitcast_dynamic-update-slice_fusion.13
  195.0 3.1 fusion
  198.4 4.6 %fusion.12 = f32[1024,512]{1,0:T(8,128)S(1)} fusion(bf16[4,512,512]{2,1,0:T(8,128)(2,1)S(1)} %bitcast.235, bf16[4,1024,512]{2,1,0:T(8,128)(2,1)} %bitcast_dynamic-update-slice_fusion, f32[4,512]{1,0:T(4,128)S(1)} %copy-done.27, f32[1024]{0:T(1024)S(1)} %add_rsqrt_fusion.3), kind=kOutput, calls=%fused_computation.22 | convolution fusion | flops 2155872256 | bytes 8400896 | tf_op jit(solution)/shard_map/btk,bkn->tn/dot_general | solution.py:125
  203.6 4.6 %convert_reduce_fusion = (f32[1024]{0:T(1024)S(1)}, f32[1024]{0:T(1024)S(1)}, bf16[1024,256]{1,0:T(8,128)(2,1)S(1)}) fusion(f32[256]{0:T(256)S(1)} %bitcast.277, f32[256]{0:T(256)S(1)} %bitcast.278, f32[256]{0:T(256)S(1)} %bitcast.249, f32[256]{0:T(256)S(1)} %bitcast.250, f32[256]{0:T(256)S(1)} %bitcast.251, f32[256]{0:T(256)S(1)} %bitcast.252, ...), kind=kLoop, calls=%fused_computation.25 | loop fusion | flops 17299456 | bytes 1612800 | tf_op jit(solution)/shard_map/reduce_sum | solution.py:170
  208.2 6.2 %all-reduce.3 = (f32[1024,1]{0,1:T(1,128)S(1)}, f32[1024,1]{0,1:T(1,128)S(1)}) all-reduce(f32[1024,1]{0,1:T(1,128)S(1)} %bitcast.243, f32[1024,1]{0,1:T(1,128)S(1)} %bitcast.242), channel_id=1, replica_groups=mesh['grp'=2,'fs'=4,'tp'=4] {'tp'}, use_global_device_ids=true, to_apply=%region_4.5 | all-reduce | flops 2048 | bytes 16384 | tf_op jit(solution)/shard_map/psum | solution.py:168
  215.7 2.0 bitcast_dynamic-update-slice_fusion.7
  217.8 1.7 bitcast_dynamic-update-slice_fusion.22
  219.5 1.7 bitcast_dynamic-update-slice_fusion.21
  222.7 5.7 %collective-permute-done.9 = bf16[1024,256]{1,0:T(8,128)(2,1)S(1)} collective-permute-done((bf16[1024,256]{1,0:T(8,128)(2,1)S(1)}, bf16[1024,256]{1,0:T(8,128)(2,1)S(1)}, u32[]{:S(2)}, u32[]{:S(2)}) %collective-permute-start.9) | collective-permute-done | bytes 524320 | tf_op jit(solution)/shard_map/ppermute | solution.py:37
  228.4 1.7 bitcast_dynamic-update-slice_fusion.20
  233.9 2.5 fusion.11
  237.2 3.3 collective-permute-done.24
  241.4 2.0 bitcast_dynamic-update-slice_fusion.11
  243.4 12.5 %collective-permute-done.30 = bf16[256,1408]{1,0:T(8,128)(2,1)S(1)} collective-permute-done((bf16[256,1408]{1,0:T(8,128)(2,1)}, bf16[256,1408]{1,0:T(8,128)(2,1)S(1)}, u32[]{:S(2)}, u32[]{:S(2)}) %collective-permute-start.30) | collective-permute-done | bytes 720928 | tf_op jit(solution)/shard_map/ppermute | solution.py:32
  256.8 4.5 %collective-permute-done.18 = bf16[1024,512]{0,1:T(8,128)(2,1)} collective-permute-done((bf16[1024,512]{0,1:T(8,128)(2,1)S(1)}, bf16[1024,512]{0,1:T(8,128)(2,1)}, u32[]{:S(2)}, u32[]{:S(2)}) %collective-permute-start.18) | collective-permute-done | bytes 1048608 | tf_op jit(solution)/shard_map/ppermute | solution.py:37
  261.3 2.1 bitcast_dynamic-update-slice_fusion.5
  263.4 7.9 %collective-permute-done.26 = bf16[256,1408]{1,0:T(8,128)(2,1)S(1)} collective-permute-done((bf16[256,1408]{1,0:T(8,128)(2,1)}, bf16[256,1408]{1,0:T(8,128)(2,1)S(1)}, u32[]{:S(2)}, u32[]{:S(2)}) %collective-permute-start.26) | collective-permute-done | bytes 720928 | tf_op jit(solution)/shard_map/ppermute | solution.py:32
  271.4 15.0 %collective-permute-done.32 = bf16[256,1408]{1,0:T(8,128)(2,1)S(1)} collective-permute-done((bf16[256,1408]{1,0:T(8,128)(2,1)}, bf16[256,1408]{1,0:T(8,128)(2,1)S(1)}, u32[]{:S(2)}, u32[]{:S(2)}) %collective-permute-start.32) | collective-permute-done | bytes 720928 | tf_op jit(solution)/shard_map/ppermute | solution.py:32
  288.3 2.3 broadcast.70
  300.3 3.1 fusion.3
  303.4 10.4 %convolution_bitcast_fusion.1 = f32[1024,1408]{1,0:T(8,128)S(1)} fusion(bf16[4,512,1408]{2,1,0:T(8,128)(2,1)} %bitcast.75, bf16[4,1024,512]{2,1,0:T(8,128)(2,1)} %constant_dynamic-update-slice_fusion.2, f32[4,512]{1,0:T(4,128)S(1)} %copy-done.26, f32[1024]{0:T(1024)S(1)} %add_rsqrt_fusion.1), kind=kOutput, calls=%fused_computation.12 | convolution fusion | flops 5913968640 | bytes 15740928 | tf_op jit(solution)/shard_map/btk,bkn->tn/dot_general | solution.py:125
  313.8 12.0 %convolution_bitcast_fusion = f32[1024,1408]{1,0:T(8,128)} fusion(bf16[4,512,1408]{2,1,0:T(8,128)(2,1)} %bitcast.85, bf16[4,1024,512]{2,1,0:T(8,128)(2,1)} %constant_dynamic-update-slice_fusion.2, f32[4,512]{1,0:T(4,128)S(1)} %copy-done.26, f32[1024]{0:T(1024)S(1)} %add_rsqrt_fusion.1), kind=kOutput, calls=%fused_computation.11 | convolution fusion | flops 5913968640 | bytes 15740928 | tf_op jit(solution)/shard_map/btk,bkn->tn/dot_general | solution.py:125
  325.8 11.1 %multiply_convert_fusion = bf16[1024,1408]{1,0:T(8,128)(2,1)S(1)} fusion(f32[1024,1408]{1,0:T(8,128)} %convolution_bitcast_fusion, f32[1024,1408]{1,0:T(8,128)S(1)} %convolution_bitcast_fusion.1, f32[1408]{0:T(1024)S(1)} %get-tuple-element.11, f32[1408]{0:T(1024)S(1)} %copy-done.20, f32[1408]{0:T(1024)S(1)} %get-tuple-element.10, f32[1408]{0:T(1024)S(1)} %copy-done.22, ...), kind=kLoop, calls=%fused_computation.10 | loop fusion | flops 23068672 | bytes 14451712 | tf_op jit(solution)/shard_map/convert_element_type | solution.py:188
  338.2 1.8 fusion.16
  340.1 1.8 fusion.18
  341.9 1.8 fusion.20
  343.8 3.2 fusion.22
  347.0 2.0 copy-done
  354.7 2.3 select_convert_fusion.1
  357.0 1.6 collective-permute-start.47
  359.1 12.8 %collective-permute-done.47 = bf16[512,512]{0,1:T(8,128)(2,1)S(1)} collective-permute-done((bf16[512,512]{0,1:T(8,128)(2,1)S(1)}, bf16[512,512]{0,1:T(8,128)(2,1)S(1)}, u32[]{:S(2)}, u32[]{:S(2)}) %collective-permute-start.47) | collective-permute-done | bytes 524320 | tf_op jit(solution)/shard_map/ppermute | solution.py:37
  371.9 10.4 %collective-permute-done.50 = bf16[512,512]{0,1:T(8,128)(2,1)S(1)} collective-permute-done((bf16[512,512]{0,1:T(8,128)(2,1)S(1)}, bf16[512,512]{0,1:T(8,128)(2,1)S(1)}, u32[]{:S(2)}, u32[]{:S(2)}) %collective-permute-start.50) | collective-permute-done | bytes 524320 | tf_op jit(solution)/shard_map/ppermute | solution.py:37
  382.3 2.2 add_bitcast_fusion.1
  384.8 6.1 %psum.23 = f32[1024,1]{0,1:T(1,128)S(1)} all-reduce(f32[1024,1]{0,1:T(1,128)S(1)} %bitcast.245), channel_id=1, replica_groups=mesh['grp'=2,'fs'=4,'tp'=4] {'tp'}, use_global_device_ids=true, to_apply=%region_7.8 | all-reduce | flops 1024 | bytes 8192 | tf_op jit(solution)/shard_map/psum | solution.py:209
  392.2 2.3 copy.36
  (267 shorter events, 78.3 us)
Async XLA Ops:
  0.0 16.4 %copy-start.2 = (bf16[1024,512]{1,0:T(8,128)(2,1)S(1)}, bf16[1024,512]{1,0:T(8,128)(2,1)}, u32[]{:S(2)}) copy-start(bf16[1024,512]{1,0:T(8,128)(2,1)} %param.15) | copy-start | bytes 3145732
  0.0 17.7 %copy-start.24 = (f32[2048]{0:T(1024)S(1)}, f32[2048]{0:T(1024)}, u32[]{:S(2)}) copy-start(f32[2048]{0:T(1024)} %param.16) | copy-start | bytes 24580
  0.0 125.5 %collective-permute-start = (bf16[1024,512]{1,0:T(8,128)(2,1)}, bf16[1024,512]{1,0:T(8,128)(2,1)}, u32[]{:S(2)}, u32[]{:S(2)}) collective-permute-start(bf16[1024,512]{1,0:T(8,128)(2,1)} %param.15), channel_id=1, source_target_pairs={{0,2},{1,3},{2,0},{3,1},{4,6},{5,7},{6,4},{7,5},{8,10},{9,11},{10,... | collective-permute-start | bytes 3145736 | tf_op jit(solution)/shard_map/ppermute | solution.py:37
  3.0 142.7 %collective-permute-start.1 = (bf16[1024,512]{1,0:T(8,128)(2,1)}, bf16[1024,512]{1,0:T(8,128)(2,1)}, u32[]{:S(2)}, u32[]{:S(2)}) collective-permute-start(bf16[1024,512]{1,0:T(8,128)(2,1)} %param.15), channel_id=1, source_target_pairs={{0,1},{1,0},{2,3},{3,2},{4,5},{5,4},{6,7},{7,6},{8,9},{9,8},{10,11... | collective-permute-start | bytes 3145736 | tf_op jit(solution)/shard_map/ppermute | solution.py:37
  4.8 18.1 %copy-start.18 = (bf16[256,512]{1,0:T(8,128)(2,1)S(1)}, bf16[256,512]{1,0:T(8,128)(2,1)}, u32[]{:S(2)}) copy-start(bf16[256,512]{1,0:T(8,128)(2,1)} %param.22) | copy-start | bytes 786436
  4.8 40.9 %collective-permute-start.3 = (bf16[256,512]{1,0:T(8,128)(2,1)}, bf16[256,512]{1,0:T(8,128)(2,1)S(1)}, u32[]{:S(2)}, u32[]{:S(2)}) collective-permute-start(bf16[256,512]{1,0:T(8,128)(2,1)} %dynamic-slice_bitcast_fusion.8), channel_id=1, source_target_pairs={{0,4},{4,8},{8,12},{12,0},{1,5},{5,9},{9,13},{13,1},{2,6},{6,10},{... | collective-permute-start | bytes 786440 | tf_op jit(solution)/shard_map/ppermute | solution.py:32
  7.9 31.6 %collective-permute-start.12 = (bf16[128,512]{1,0:T(8,128)(2,1)}, bf16[128,512]{1,0:T(8,128)(2,1)S(1)}, u32[]{:S(2)}, u32[]{:S(2)}) collective-permute-start(bf16[128,512]{1,0:T(8,128)(2,1)} %dynamic-slice_bitcast_fusion.9), channel_id=1, source_target_pairs={{0,4},{4,8},{8,12},{12,0},{1,5},{5,9},{9,13},{13,1},{2,6},{6,10},{... | collective-permute-start | bytes 393224 | tf_op jit(solution)/shard_map/ppermute | solution.py:32
  11.5 75.1 %collective-permute-start.21 = (bf16[256,1408]{1,0:T(8,128)(2,1)}, bf16[256,1408]{1,0:T(8,128)(2,1)}, u32[]{:S(2)}, u32[]{:S(2)}) collective-permute-start(bf16[256,1408]{1,0:T(8,128)(2,1)} %dynamic-slice_bitcast_fusion.1), channel_id=1, source_target_pairs={{0,4},{4,8},{8,12},{12,0},{1,5},{5,9},{9,13},{13,1},{2,6},{6,10},{... | collective-permute-start | bytes 2162696 | tf_op jit(solution)/shard_map/ppermute | solution.py:32
  33.4 21.5 %copy-start.6 = (bf16[8,256,512]{2,1,0:T(8,128)(2,1)S(1)}, bf16[8,256,512]{2,1,0:T(8,128)(2,1)}, u32[]{:S(2)}) copy-start(bf16[8,256,512]{2,1,0:T(8,128)(2,1)} %copy-done.5) | copy-start | bytes 6291460
  36.8 33.9 %copy-start.17 = (bf16[256,1408]{1,0:T(8,128)(2,1)S(1)}, bf16[256,1408]{1,0:T(8,128)(2,1)}, u32[]{:S(2)}) copy-start(bf16[256,1408]{1,0:T(8,128)(2,1)} %dynamic-slice_bitcast_fusion) | copy-start | bytes 2162692
  39.6 5.1 %collective-permute-start.13 = (bf16[128,512]{1,0:T(8,128)(2,1)S(1)}, bf16[128,512]{1,0:T(8,128)(2,1)S(1)}, u32[]{:S(2)}, u32[]{:S(2)}) collective-permute-start(bf16[128,512]{1,0:T(8,128)(2,1)S(1)} %collective-permute-done.12), channel_id=1, source_target_pairs={{0,16},{16,0},{1,17},{17,1},{2,18},{18,2},{3,19},{19,3},{4,20},{20... | collective-permute-start | bytes 393224 | tf_op jit(solution)/shard_map/ppermute | solution.py:32
  44.6 8.2 %collective-permute-start.14 = (bf16[128,512]{1,0:T(8,128)(2,1)S(1)}, bf16[128,512]{1,0:T(8,128)(2,1)S(1)}, u32[]{:S(2)}, u32[]{:S(2)}) collective-permute-start(bf16[128,512]{1,0:T(8,128)(2,1)S(1)} %collective-permute-done.12), channel_id=1, source_target_pairs={{0,4},{4,8},{8,12},{12,0},{1,5},{5,9},{9,13},{13,1},{2,6},{6,10},{... | collective-permute-start | bytes 393224 | tf_op jit(solution)/shard_map/ppermute | solution.py:32
  45.7 12.6 %collective-permute-start.33 = (bf16[352,512]{1,0:T(8,128)(2,1)S(1)}, bf16[352,512]{1,0:T(8,128)(2,1)S(1)}, u32[]{:S(2)}, u32[]{:S(2)}) collective-permute-start(bf16[352,512]{1,0:T(8,128)(2,1)S(1)} %get-tuple-element.27), channel_id=1, source_target_pairs={{0,4},{4,8},{8,12},{12,0},{1,5},{5,9},{9,13},{13,1},{2,6},{6,10},{... | collective-permute-start | bytes 1081352 | tf_op jit(solution)/shard_map/ppermute | solution.py:32
  52.8 17.9 %collective-permute-start.4 = (bf16[256,512]{1,0:T(8,128)(2,1)S(1)}, bf16[256,512]{1,0:T(8,128)(2,1)S(1)}, u32[]{:S(2)}, u32[]{:S(2)}) collective-permute-start(bf16[256,512]{1,0:T(8,128)(2,1)S(1)} %collective-permute-done.3), channel_id=1, source_target_pairs={{0,16},{16,0},{1,17},{17,1},{2,18},{18,2},{3,19},{19,3},{4,20},{20... | collective-permute-start | bytes 786440 | tf_op jit(solution)/shard_map/ppermute | solution.py:32
  58.3 5.0 %collective-permute-start.15 = (bf16[128,512]{1,0:T(8,128)(2,1)S(1)}, bf16[128,512]{1,0:T(8,128)(2,1)S(1)}, u32[]{:S(2)}, u32[]{:S(2)}) collective-permute-start(bf16[128,512]{1,0:T(8,128)(2,1)S(1)} %collective-permute-done.14), channel_id=1, source_target_pairs={{0,16},{16,0},{1,17},{17,1},{2,18},{18,2},{3,19},{19,3},{4,20},{20... | collective-permute-start | bytes 393224 | tf_op jit(solution)/shard_map/ppermute | solution.py:32
  63.3 6.8 %collective-permute-start.16 = (bf16[128,512]{1,0:T(8,128)(2,1)S(1)}, bf16[128,512]{1,0:T(8,128)(2,1)S(1)}, u32[]{:S(2)}, u32[]{:S(2)}) collective-permute-start(bf16[128,512]{1,0:T(8,128)(2,1)S(1)} %collective-permute-done.14), channel_id=1, source_target_pairs={{0,4},{4,8},{8,12},{12,0},{1,5},{5,9},{9,13},{13,1},{2,6},{6,10},{... | collective-permute-start | bytes 393224 | tf_op jit(solution)/shard_map/ppermute | solution.py:32
  70.1 11.0 %collective-permute-start.5 = (bf16[256,512]{1,0:T(8,128)(2,1)S(1)}, bf16[256,512]{1,0:T(8,128)(2,1)S(1)}, u32[]{:S(2)}, u32[]{:S(2)}) collective-permute-start(bf16[256,512]{1,0:T(8,128)(2,1)S(1)} %collective-permute-done.3), channel_id=1, source_target_pairs={{0,4},{4,8},{8,12},{12,0},{1,5},{5,9},{9,13},{13,1},{2,6},{6,10},{... | collective-permute-start | bytes 786440 | tf_op jit(solution)/shard_map/ppermute | solution.py:32
  70.7 29.0 %collective-permute-start.27 = (bf16[256,1408]{1,0:T(8,128)(2,1)S(1)}, bf16[256,1408]{1,0:T(8,128)(2,1)S(1)}, u32[]{:S(2)}, u32[]{:S(2)}) collective-permute-start(bf16[256,1408]{1,0:T(8,128)(2,1)S(1)} %copy-done.17), channel_id=1, source_target_pairs={{0,4},{4,8},{8,12},{12,0},{1,5},{5,9},{9,13},{13,1},{2,6},{6,10},{... | collective-permute-start | bytes 2162696 | tf_op jit(solution)/shard_map/ppermute | solution.py:32
  81.0 5.0 %collective-permute-start.17 = (bf16[128,512]{1,0:T(8,128)(2,1)S(1)}, bf16[128,512]{1,0:T(8,128)(2,1)S(1)}, u32[]{:S(2)}, u32[]{:S(2)}) collective-permute-start(bf16[128,512]{1,0:T(8,128)(2,1)S(1)} %collective-permute-done.16), channel_id=1, source_target_pairs={{0,16},{16,0},{1,17},{17,1},{2,18},{18,2},{3,19},{19,3},{4,20},{20... | collective-permute-start | bytes 393224 | tf_op jit(solution)/shard_map/ppermute | solution.py:32
  86.0 13.7 %collective-permute-start.35 = (bf16[352,512]{1,0:T(8,128)(2,1)S(1)}, bf16[352,512]{1,0:T(8,128)(2,1)S(1)}, u32[]{:S(2)}, u32[]{:S(2)}) collective-permute-start(bf16[352,512]{1,0:T(8,128)(2,1)S(1)} %get-tuple-element.26), channel_id=1, source_target_pairs={{0,4},{4,8},{8,12},{12,0},{1,5},{5,9},{9,13},{13,1},{2,6},{6,10},{... | collective-permute-start | bytes 1081352 | tf_op jit(solution)/shard_map/ppermute | solution.py:32
  86.7 15.5 %collective-permute-start.34 = (bf16[352,512]{1,0:T(8,128)(2,1)S(1)}, bf16[352,512]{1,0:T(8,128)(2,1)S(1)}, u32[]{:S(2)}, u32[]{:S(2)}) collective-permute-start(bf16[352,512]{1,0:T(8,128)(2,1)S(1)} %collective-permute-done.33), channel_id=1, source_target_pairs={{0,16},{16,0},{1,17},{17,1},{2,18},{18,2},{3,19},{19,3},{4,20},{20... | collective-permute-start | bytes 1081352 | tf_op jit(solution)/shard_map/ppermute | solution.py:32
  99.7 13.1 %collective-permute-start.37 = (bf16[352,512]{1,0:T(8,128)(2,1)S(1)}, bf16[352,512]{1,0:T(8,128)(2,1)S(1)}, u32[]{:S(2)}, u32[]{:S(2)}) collective-permute-start(bf16[352,512]{1,0:T(8,128)(2,1)S(1)} %collective-permute-done.33), channel_id=1, source_target_pairs={{0,4},{4,8},{8,12},{12,0},{1,5},{5,9},{9,13},{13,1},{2,6},{6,10},{... | collective-permute-start | bytes 1081352 | tf_op jit(solution)/shard_map/ppermute | solution.py:32
  99.7 14.8 %collective-permute-start.36 = (bf16[352,512]{1,0:T(8,128)(2,1)S(1)}, bf16[352,512]{1,0:T(8,128)(2,1)S(1)}, u32[]{:S(2)}, u32[]{:S(2)}) collective-permute-start(bf16[352,512]{1,0:T(8,128)(2,1)S(1)} %collective-permute-done.35), channel_id=1, source_target_pairs={{0,16},{16,0},{1,17},{17,1},{2,18},{18,2},{3,19},{19,3},{4,20},{20... | collective-permute-start | bytes 1081352 | tf_op jit(solution)/shard_map/ppermute | solution.py:32
  102.1 46.4 %collective-permute-start.39 = (bf16[352,512]{1,0:T(8,128)(2,1)S(1)}, bf16[352,512]{1,0:T(8,128)(2,1)S(1)}, u32[]{:S(2)}, u32[]{:S(2)}) collective-permute-start(bf16[352,512]{1,0:T(8,128)(2,1)S(1)} %collective-permute-done.35), channel_id=1, source_target_pairs={{0,4},{4,8},{8,12},{12,0},{1,5},{5,9},{9,13},{13,1},{2,6},{6,10},{... | collective-permute-start | bytes 1081352 | tf_op jit(solution)/shard_map/ppermute | solution.py:32
  112.8 9.2 %collective-permute-start.6 = (bf16[256,512]{1,0:T(8,128)(2,1)S(1)}, bf16[256,512]{1,0:T(8,128)(2,1)S(1)}, u32[]{:S(2)}, u32[]{:S(2)}) collective-permute-start(bf16[256,512]{1,0:T(8,128)(2,1)S(1)} %collective-permute-done.5), channel_id=1, source_target_pairs={{0,16},{16,0},{1,17},{17,1},{2,18},{18,2},{3,19},{19,3},{4,20},{20... | collective-permute-start | bytes 786440 | tf_op jit(solution)/shard_map/ppermute | solution.py:32
  114.5 11.0 %collective-permute-start.7 = (bf16[256,512]{1,0:T(8,128)(2,1)S(1)}, bf16[256,512]{1,0:T(8,128)(2,1)S(1)}, u32[]{:S(2)}, u32[]{:S(2)}) collective-permute-start(bf16[256,512]{1,0:T(8,128)(2,1)S(1)} %collective-permute-done.5), channel_id=1, source_target_pairs={{0,4},{4,8},{8,12},{12,0},{1,5},{5,9},{9,13},{13,1},{2,6},{6,10},{... | collective-permute-start | bytes 786440 | tf_op jit(solution)/shard_map/ppermute | solution.py:32
  114.6 54.5 %copy-start.11 = (bf16[4,352,512]{2,1,0:T(8,128)(2,1)}, bf16[4,352,512]{2,1,0:T(8,128)(2,1)S(1)}, u32[]{:S(2)}) copy-start(bf16[4,352,512]{2,1,0:T(8,128)(2,1)S(1)} %bitcast_dynamic-update-slice_fusion.28) | copy-start | bytes 4325380
  122.0 47.9 %collective-permute-start.22 = (bf16[256,1408]{1,0:T(8,128)(2,1)}, bf16[256,1408]{1,0:T(8,128)(2,1)S(1)}, u32[]{:S(2)}, u32[]{:S(2)}) collective-permute-start(bf16[256,1408]{1,0:T(8,128)(2,1)} %collective-permute-done.21), channel_id=1, source_target_pairs={{0,16},{16,0},{1,17},{17,1},{2,18},{18,2},{3,19},{19,3},{4,20},{20... | collective-permute-start | bytes 2162696 | tf_op jit(solution)/shard_map/ppermute | solution.py:32
  125.5 64.4 %collective-permute-start.23 = (bf16[256,1408]{1,0:T(8,128)(2,1)}, bf16[256,1408]{1,0:T(8,128)(2,1)}, u32[]{:S(2)}, u32[]{:S(2)}) collective-permute-start(bf16[256,1408]{1,0:T(8,128)(2,1)} %collective-permute-done.21), channel_id=1, source_target_pairs={{0,4},{4,8},{8,12},{12,0},{1,5},{5,9},{9,13},{13,1},{2,6},{6,10},{... | collective-permute-start | bytes 2162696 | tf_op jit(solution)/shard_map/ppermute | solution.py:32
  125.5 18.6 %collective-permute-start.8 = (bf16[256,512]{1,0:T(8,128)(2,1)S(1)}, bf16[256,512]{1,0:T(8,128)(2,1)S(1)}, u32[]{:S(2)}, u32[]{:S(2)}) collective-permute-start(bf16[256,512]{1,0:T(8,128)(2,1)S(1)} %collective-permute-done.7), channel_id=1, source_target_pairs={{0,16},{16,0},{1,17},{17,1},{2,18},{18,2},{3,19},{19,3},{4,20},{20... | collective-permute-start | bytes 786440 | tf_op jit(solution)/shard_map/ppermute | solution.py:32
  144.1 11.3 %collective-permute-start.38 = (bf16[352,512]{1,0:T(8,128)(2,1)S(1)}, bf16[352,512]{1,0:T(8,128)(2,1)S(1)}, u32[]{:S(2)}, u32[]{:S(2)}) collective-permute-start(bf16[352,512]{1,0:T(8,128)(2,1)S(1)} %collective-permute-done.37), channel_id=1, source_target_pairs={{0,16},{16,0},{1,17},{17,1},{2,18},{18,2},{3,19},{19,3},{4,20},{20... | collective-permute-start | bytes 1081352 | tf_op jit(solution)/shard_map/ppermute | solution.py:32
  145.7 46.8 %collective-permute-start.28 = (bf16[256,1408]{1,0:T(8,128)(2,1)S(1)}, bf16[256,1408]{1,0:T(8,128)(2,1)S(1)}, u32[]{:S(2)}, u32[]{:S(2)}) collective-permute-start(bf16[256,1408]{1,0:T(8,128)(2,1)S(1)} %collective-permute-done.27), channel_id=1, source_target_pairs={{0,16},{16,0},{1,17},{17,1},{2,18},{18,2},{3,19},{19,3},{4,20},{20... | collective-permute-start | bytes 2162696 | tf_op jit(solution)/shard_map/ppermute | solution.py:32
  148.5 19.2 %collective-permute-start.41 = (bf16[352,512]{1,0:T(8,128)(2,1)S(1)}, bf16[352,512]{1,0:T(8,128)(2,1)S(1)}, u32[]{:S(2)}, u32[]{:S(2)}) collective-permute-start(bf16[352,512]{1,0:T(8,128)(2,1)S(1)} %collective-permute-done.37), channel_id=1, source_target_pairs={{0,4},{4,8},{8,12},{12,0},{1,5},{5,9},{9,13},{13,1},{2,6},{6,10},{... | collective-permute-start | bytes 1081352 | tf_op jit(solution)/shard_map/ppermute | solution.py:32
  155.4 12.2 %collective-permute-start.40 = (bf16[352,512]{1,0:T(8,128)(2,1)S(1)}, bf16[352,512]{1,0:T(8,128)(2,1)S(1)}, u32[]{:S(2)}, u32[]{:S(2)}) collective-permute-start(bf16[352,512]{1,0:T(8,128)(2,1)S(1)} %collective-permute-done.39), channel_id=1, source_target_pairs={{0,16},{16,0},{1,17},{17,1},{2,18},{18,2},{3,19},{19,3},{4,20},{20... | collective-permute-start | bytes 1081352 | tf_op jit(solution)/shard_map/ppermute | solution.py:32
  167.6 24.9 %collective-permute-start.29 = (bf16[256,1408]{1,0:T(8,128)(2,1)S(1)}, bf16[256,1408]{1,0:T(8,128)(2,1)}, u32[]{:S(2)}, u32[]{:S(2)}) collective-permute-start(bf16[256,1408]{1,0:T(8,128)(2,1)S(1)} %collective-permute-done.27), channel_id=1, source_target_pairs={{0,4},{4,8},{8,12},{12,0},{1,5},{5,9},{9,13},{13,1},{2,6},{6,10},{... | collective-permute-start | bytes 2162696 | tf_op jit(solution)/shard_map/ppermute | solution.py:32
  167.7 20.7 %collective-permute-start.43 = (bf16[352,512]{1,0:T(8,128)(2,1)S(1)}, bf16[352,512]{1,0:T(8,128)(2,1)}, u32[]{:S(2)}, u32[]{:S(2)}) collective-permute-start(bf16[352,512]{1,0:T(8,128)(2,1)S(1)} %collective-permute-done.39), channel_id=1, source_target_pairs={{0,4},{4,8},{8,12},{12,0},{1,5},{5,9},{9,13},{13,1},{2,6},{6,10},{... | collective-permute-start | bytes 1081352 | tf_op jit(solution)/shard_map/ppermute | solution.py:32
  169.9 24.1 %collective-permute-start.2 = (bf16[1024,512]{1,0:T(8,128)(2,1)}, bf16[1024,512]{1,0:T(8,128)(2,1)S(1)}, u32[]{:S(2)}, u32[]{:S(2)}) collective-permute-start(bf16[1024,512]{1,0:T(8,128)(2,1)} %collective-permute-done), channel_id=1, source_target_pairs={{0,1},{1,0},{2,3},{3,2},{4,5},{5,4},{6,7},{7,6},{8,9},{9,8},{10,11... | collective-permute-start | bytes 3145736 | tf_op jit(solution)/shard_map/ppermute | solution.py:37
  188.4 29.3 %collective-permute-start.42 = (bf16[352,512]{1,0:T(8,128)(2,1)S(1)}, bf16[352,512]{1,0:T(8,128)(2,1)}, u32[]{:S(2)}, u32[]{:S(2)}) collective-permute-start(bf16[352,512]{1,0:T(8,128)(2,1)S(1)} %collective-permute-done.41), channel_id=1, source_target_pairs={{0,16},{16,0},{1,17},{17,1},{2,18},{18,2},{3,19},{19,3},{4,20},{20... | collective-permute-start | bytes 1081352 | tf_op jit(solution)/shard_map/ppermute | solution.py:32
  189.9 31.3 %collective-permute-start.44 = (bf16[352,512]{1,0:T(8,128)(2,1)}, bf16[352,512]{1,0:T(8,128)(2,1)}, u32[]{:S(2)}, u32[]{:S(2)}) collective-permute-start(bf16[352,512]{1,0:T(8,128)(2,1)} %collective-permute-done.43), channel_id=1, source_target_pairs={{0,16},{16,0},{1,17},{17,1},{2,18},{18,2},{3,19},{19,3},{4,20},{20... | collective-permute-start | bytes 1081352 | tf_op jit(solution)/shard_map/ppermute | solution.py:32
  192.5 37.7 %collective-permute-start.25 = (bf16[256,1408]{1,0:T(8,128)(2,1)}, bf16[256,1408]{1,0:T(8,128)(2,1)}, u32[]{:S(2)}, u32[]{:S(2)}) collective-permute-start(bf16[256,1408]{1,0:T(8,128)(2,1)} %collective-permute-done.23), channel_id=1, source_target_pairs={{0,4},{4,8},{8,12},{12,0},{1,5},{5,9},{9,13},{13,1},{2,6},{6,10},{... | collective-permute-start | bytes 2162696 | tf_op jit(solution)/shard_map/ppermute | solution.py:32
  192.5 39.2 %collective-permute-start.31 = (bf16[256,1408]{1,0:T(8,128)(2,1)}, bf16[256,1408]{1,0:T(8,128)(2,1)}, u32[]{:S(2)}, u32[]{:S(2)}) collective-permute-start(bf16[256,1408]{1,0:T(8,128)(2,1)} %collective-permute-done.29), channel_id=1, source_target_pairs={{0,4},{4,8},{8,12},{12,0},{1,5},{5,9},{9,13},{13,1},{2,6},{6,10},{... | collective-permute-start | bytes 2162696 | tf_op jit(solution)/shard_map/ppermute | solution.py:32
  214.7 19.2 %copy-start.15 = (bf16[1024,512]{0,1:T(8,128)(2,1)S(1)}, bf16[1024,512]{0,1:T(8,128)(2,1)}, u32[]{:S(2)}) copy-start(bf16[1024,512]{0,1:T(8,128)(2,1)} %copy.26) | copy-start | bytes 3145732
  215.1 13.2 %collective-permute-start.9 = (bf16[1024,256]{1,0:T(8,128)(2,1)S(1)}, bf16[1024,256]{1,0:T(8,128)(2,1)S(1)}, u32[]{:S(2)}, u32[]{:S(2)}) collective-permute-start(bf16[1024,256]{1,0:T(8,128)(2,1)S(1)} %get-tuple-element.16), channel_id=1, source_target_pairs={{0,2},{1,3},{2,0},{3,1},{4,6},{5,7},{6,4},{7,5},{8,10},{9,11},{10,... | collective-permute-start | bytes 1572872 | tf_op jit(solution)/shard_map/ppermute | solution.py:37
  219.5 12.8 %collective-permute-start.10 = (bf16[1024,256]{1,0:T(8,128)(2,1)S(1)}, bf16[1024,256]{1,0:T(8,128)(2,1)S(1)}, u32[]{:S(2)}, u32[]{:S(2)}) collective-permute-start(bf16[1024,256]{1,0:T(8,128)(2,1)S(1)} %get-tuple-element.16), channel_id=1, source_target_pairs={{0,1},{1,0},{2,3},{3,2},{4,5},{5,4},{6,7},{7,6},{8,9},{9,8},{10,11... | collective-permute-start | bytes 1572872 | tf_op jit(solution)/shard_map/ppermute | solution.py:37
  221.2 19.2 %collective-permute-start.24 = (bf16[256,1408]{1,0:T(8,128)(2,1)}, bf16[256,1408]{1,0:T(8,128)(2,1)S(1)}, u32[]{:S(2)}, u32[]{:S(2)}) collective-permute-start(bf16[256,1408]{1,0:T(8,128)(2,1)} %collective-permute-done.23), channel_id=1, source_target_pairs={{0,16},{16,0},{1,17},{17,1},{2,18},{18,2},{3,19},{19,3},{4,20},{20... | collective-permute-start | bytes 2162696 | tf_op jit(solution)/shard_map/ppermute | solution.py:32
  228.4 5.4 %collective-permute-start.11 = (bf16[1024,256]{1,0:T(8,128)(2,1)S(1)}, bf16[1024,256]{1,0:T(8,128)(2,1)S(1)}, u32[]{:S(2)}, u32[]{:S(2)}) collective-permute-start(bf16[1024,256]{1,0:T(8,128)(2,1)S(1)} %collective-permute-done.9), channel_id=1, source_target_pairs={{0,1},{1,0},{2,3},{3,2},{4,5},{5,4},{6,7},{7,6},{8,9},{9,8},{10,11... | collective-permute-start | bytes 1572872 | tf_op jit(solution)/shard_map/ppermute | solution.py:37
  230.2 25.7 %collective-permute-start.30 = (bf16[256,1408]{1,0:T(8,128)(2,1)}, bf16[256,1408]{1,0:T(8,128)(2,1)S(1)}, u32[]{:S(2)}, u32[]{:S(2)}) collective-permute-start(bf16[256,1408]{1,0:T(8,128)(2,1)} %collective-permute-done.29), channel_id=1, source_target_pairs={{0,16},{16,0},{1,17},{17,1},{2,18},{18,2},{3,19},{19,3},{4,20},{20... | collective-permute-start | bytes 2162696 | tf_op jit(solution)/shard_map/ppermute | solution.py:32
  231.7 39.6 %collective-permute-start.26 = (bf16[256,1408]{1,0:T(8,128)(2,1)}, bf16[256,1408]{1,0:T(8,128)(2,1)S(1)}, u32[]{:S(2)}, u32[]{:S(2)}) collective-permute-start(bf16[256,1408]{1,0:T(8,128)(2,1)} %collective-permute-done.25), channel_id=1, source_target_pairs={{0,16},{16,0},{1,17},{17,1},{2,18},{18,2},{3,19},{19,3},{4,20},{20... | collective-permute-start | bytes 2162696 | tf_op jit(solution)/shard_map/ppermute | solution.py:32
  232.3 54.1 %collective-permute-start.32 = (bf16[256,1408]{1,0:T(8,128)(2,1)}, bf16[256,1408]{1,0:T(8,128)(2,1)S(1)}, u32[]{:S(2)}, u32[]{:S(2)}) collective-permute-start(bf16[256,1408]{1,0:T(8,128)(2,1)} %collective-permute-done.31), channel_id=1, source_target_pairs={{0,16},{16,0},{1,17},{17,1},{2,18},{18,2},{3,19},{19,3},{4,20},{20... | collective-permute-start | bytes 2162696 | tf_op jit(solution)/shard_map/ppermute | solution.py:32
  236.4 24.9 %collective-permute-start.18 = (bf16[1024,512]{0,1:T(8,128)(2,1)S(1)}, bf16[1024,512]{0,1:T(8,128)(2,1)}, u32[]{:S(2)}, u32[]{:S(2)}) collective-permute-start(bf16[1024,512]{0,1:T(8,128)(2,1)S(1)} %fusion.11), channel_id=1, source_target_pairs={{0,2},{1,3},{2,0},{3,1},{4,6},{5,7},{6,4},{7,5},{8,10},{9,11},{10,... | collective-permute-start | bytes 3145736 | tf_op jit(solution)/shard_map/ppermute | solution.py:37
  256.8 36.3 %collective-permute-start.19 = (bf16[1024,512]{0,1:T(8,128)(2,1)S(1)}, bf16[1024,512]{0,1:T(8,128)(2,1)S(1)}, u32[]{:S(2)}, u32[]{:S(2)}) collective-permute-start(bf16[1024,512]{0,1:T(8,128)(2,1)S(1)} %fusion.11), channel_id=1, source_target_pairs={{0,1},{1,0},{2,3},{3,2},{4,5},{5,4},{6,7},{7,6},{8,9},{9,8},{10,11... | collective-permute-start | bytes 3145736 | tf_op jit(solution)/shard_map/ppermute | solution.py:37
  261.3 36.4 %collective-permute-start.20 = (bf16[1024,512]{0,1:T(8,128)(2,1)}, bf16[1024,512]{0,1:T(8,128)(2,1)}, u32[]{:S(2)}, u32[]{:S(2)}) collective-permute-start(bf16[1024,512]{0,1:T(8,128)(2,1)} %collective-permute-done.18), channel_id=1, source_target_pairs={{0,1},{1,0},{2,3},{3,2},{4,5},{5,4},{6,7},{7,6},{8,9},{9,8},{10,11... | collective-permute-start | bytes 3145736 | tf_op jit(solution)/shard_map/ppermute | solution.py:37
  350.4 2.1 collective-permute-start.45
  350.4 2.9 collective-permute-start.46
  350.9 3.1 collective-permute-start.48
  350.9 3.9 collective-permute-start.49
  351.4 30.9 %copy-start.1 = (bf16[4,1,1024,512]{2,3,1,0:T(8,128)(2,1)S(1)}, bf16[4,1,1024,512]{2,3,1,0:T(8,128)(2,1)}, u32[]{:S(2)}) copy-start(bf16[4,1,1024,512]{2,3,1,0:T(8,128)(2,1)} %copy-done) | copy-start | bytes 12582916
  352.5 19.4 %copy-start.7 = (bf16[512,512]{0,1:T(8,128)(2,1)}, bf16[512,512]{0,1:T(8,128)(2,1)S(1)}, u32[]{:S(2)}) copy-start(bf16[512,512]{0,1:T(8,128)(2,1)S(1)} %collective-permute-done.45) | copy-start | bytes 1572868
  353.2 18.6 %copy-start.8 = (bf16[512,512]{0,1:T(8,128)(2,1)}, bf16[512,512]{0,1:T(8,128)(2,1)S(1)}, u32[]{:S(2)}) copy-start(bf16[512,512]{0,1:T(8,128)(2,1)S(1)} %collective-permute-done.46) | copy-start | bytes 1572868
  354.0 17.9 %copy-start.9 = (bf16[512,512]{0,1:T(8,128)(2,1)}, bf16[512,512]{0,1:T(8,128)(2,1)S(1)}, u32[]{:S(2)}) copy-start(bf16[512,512]{0,1:T(8,128)(2,1)S(1)} %collective-permute-done.48) | copy-start | bytes 1572868
  354.7 17.1 %copy-start.10 = (bf16[512,512]{0,1:T(8,128)(2,1)}, bf16[512,512]{0,1:T(8,128)(2,1)S(1)}, u32[]{:S(2)}) copy-start(bf16[512,512]{0,1:T(8,128)(2,1)S(1)} %collective-permute-done.49) | copy-start | bytes 1572868
  357.0 14.9 %collective-permute-start.47 = (bf16[512,512]{0,1:T(8,128)(2,1)S(1)}, bf16[512,512]{0,1:T(8,128)(2,1)S(1)}, u32[]{:S(2)}, u32[]{:S(2)}) collective-permute-start(bf16[512,512]{0,1:T(8,128)(2,1)S(1)} %get-tuple-element.20), channel_id=1, source_target_pairs={{0,2},{1,3},{2,0},{3,1},{4,6},{5,7},{6,4},{7,5},{8,10},{9,11},{10,... | collective-permute-start | bytes 1572872 | tf_op jit(solution)/shard_map/ppermute | solution.py:37
  358.6 32.3 %copy-start.61 = (f32[512]{0:T(512)S(1)}, f32[512]{0:T(512)}, u32[]{:S(2)}) copy-start(f32[512]{0:T(512)} %param.29) | copy-start | bytes 6148
  358.6 23.7 %collective-permute-start.50 = (bf16[512,512]{0,1:T(8,128)(2,1)S(1)}, bf16[512,512]{0,1:T(8,128)(2,1)S(1)}, u32[]{:S(2)}, u32[]{:S(2)}) collective-permute-start(bf16[512,512]{0,1:T(8,128)(2,1)S(1)} %get-tuple-element.21), channel_id=1, source_target_pairs={{0,2},{1,3},{2,0},{3,1},{4,6},{5,7},{6,4},{7,5},{8,10},{9,11},{10,... | collective-permute-start | bytes 1572872 | tf_op jit(solution)/shard_map/ppermute | solution.py:37
  (49 other events, 269.0 us)
